TPU v7x, 256 devices: a 4x2x16 block of a 4x16x16 slice. The times are simulated.
256 devices in a mesh: grp: 2 (over y), sp: 16 (over z), tp: 8 (over x, core).
Axes of the slice: x: 4, y: 2, z: 16, core: 2. Of those that a mesh axis runs over, the one named last changes fastest.
The devices are a block of a 4x16x16 slice.
Arguments:
- stream: bfloat16 [98304, 4096], P(('grp', 'sp', 'tp')), parts along dimension 0, may hold values from -6 to 6
- norm_gain: float32 [2, 4096], replicated, may hold values from 0.1 to 1.9
- mix_weight: bfloat16 [2, 4, 1024, 1024], P(None, None, 'sp', 'tp'), may hold values from -0.1875 to 0.1875
- branch_scale: float32 [2, 4096], replicated, may hold values from 0.1 to 1.9
Outputs:
- result: bfloat16 [98304, 4096], P(('grp', 'sp', 'tp')), parts along dimension 0
There are 2 independent parts, one for each index of `grp`. A program takes and returns all parts, laid end to end along the dimension named above; an argument that names none is the same for every part. Nothing has to cross between parts.
All inputs are finite; a program needn't handle non-finite values.
Results may differ from a plain program's by a relative error of at most 0.0056.
Values may be sent and summed in bfloat16 or wider, within the bound.
A program may use at most 128 MiB of HBM per device.

v0:
```python
import jax
import jax.numpy as jnp
from jax import lax
from jax.sharding import PartitionSpec as P

GW = 1024
G = 4
LAYERS = 2


epsilon = 1e-06
window_lengths = (2, 4, 8, 16)
halo_rows = 15


def from_behind(block, axis, distance):
    devices = range(lax.axis_size(axis))
    route = [(i - distance, i) for i in devices if i - distance in devices]
    return lax.ppermute(block, axis, route)


def joined_along(pieces, dim):
    pieces = jnp.moveaxis(pieces, 0, dim)
    lengths = pieces.shape
    return pieces.reshape(*lengths[:dim], lengths[dim] * lengths[dim + 1], *lengths[dim + 2 :])


def sent_to_all(x, axis):
    length = lax.axis_size(axis)
    return lax.all_to_all(jnp.broadcast_to(x[None], (length, *x.shape)), axis, 0, 0, tiled=True)


def collect(x, axis, dim):
    return joined_along(sent_to_all(x, axis), dim)


def per_device(stream, norm_gain, mix_weight, branch_scale):
    row_count = stream.shape[0]
    feature_width = stream.shape[1]
    offset = lax.axis_index(("sp", "tp")) * row_count
    counts_base = (offset + lax.iota(jnp.int32, row_count)).astype(jnp.float32) + 1.0
    residual = stream.astype(jnp.float32)
    for layer_idx in range(LAYERS):
        scale_rows = lax.rsqrt(jnp.mean(residual * residual, axis=1, keepdims=True) + epsilon)
        normed = (residual * scale_rows * norm_gain[layer_idx]).astype(jnp.bfloat16)
        earlier = from_behind(normed[row_count - halo_rows :], ("sp", "tp"), 1)
        extended = jnp.concatenate([earlier, normed], axis=0).astype(jnp.float32)
        pieces = []
        for group_idx in range(G):
            window_len = window_lengths[group_idx]
            segment = extended[:, group_idx * GW : (group_idx + 1) * GW]
            own_rows = segment[halo_rows:]
            running = own_rows
            for back_step in range(1, window_len):
                running = (
                    running + segment[halo_rows - back_step : halo_rows - back_step + row_count]
                )
            window_mean = running / jnp.minimum(counts_base, float(window_len))[:, None]
            pieces.append((window_mean - own_rows).astype(jnp.bfloat16))
        pooled = jnp.stack(pieces, axis=1)
        weight_shard = mix_weight[layer_idx]
        full_rows = collect(weight_shard, "sp", 1)
        mixed_out = jnp.einsum(
            "rgc,gcn->rgn",
            pooled,
            lax.all_gather(full_rows, "tp", axis=2, tiled=True),
            preferred_element_type=jnp.float32,
        )
        residual = residual + mixed_out.reshape(row_count, feature_width) * branch_scale[layer_idx]
    return residual.astype(jnp.bfloat16)


def solution(mesh):
    return jax.shard_map(
        per_device,
        mesh=mesh,
        in_specs=(P(("grp", "sp", "tp"), None), P(), P(None, None, "sp", "tp"), P()),
        out_specs=P(("grp", "sp", "tp"), None),
        check_vma=False,
    )
```

profile of v0, /device:TPU:33, one launch (start us, length us, event | category | flops | bytes accessed | tf_op | source)
XLA Modules:
  0.0 229.3 jit_solution(12822001037860567513)
XLA Ops:
  6.5 0.0 all-gather.3.cloned.1.call-start
  6.6 0.9 slice_bitcast_fusion.1
  7.4 0.2 broadcast_in_dim.9
  7.7 69.6 %all_to_all.10 = bf16[16,4,64,128]{3,2,1,0:T(8,128)(2,1)S(1)} all-to-all(bf16[16,4,64,128]{3,2,1,0:T(8,128)(2,1)S(1)} %broadcast_in_dim.9), channel_id=1, replica_groups=mesh['grp'=2,'sp'=16,'tp'=8] {'sp'}, dimensions={0} | all-to-all | bytes 2097152 | tf_op jit(solution)/shard_map/all_to_all | solution.py:30
  77.2 1.1 copy.7
  78.3 0.1 all-gather.3.cloned.1.call-update
  78.4 0.1 all-gather.5.cloned.1.call-start
  78.5 0.2 broadcast_in_dim.11
  78.7 57.7 %all_to_all.11 = bf16[16,4,64,128]{3,2,1,0:T(8,128)(2,1)S(1)} all-to-all(bf16[16,4,64,128]{3,2,1,0:T(8,128)(2,1)S(1)} %broadcast_in_dim.11), channel_id=1, replica_groups=mesh['grp'=2,'sp'=16,'tp'=8] {'sp'}, dimensions={0} | all-to-all | bytes 2097152 | tf_op jit(solution)/shard_map/all_to_all | solution.py:30
  136.5 0.0 copy-start.1
  136.5 1.1 copy.9
  137.5 0.1 all-gather.5.cloned.1.call-update
  137.6 1.2 copy-done.1
  138.8 0.0 copy-start.3
  138.8 0.7 fusion
  139.5 0.1 copy-done.3
  139.6 0.0 copy-start.4
  139.6 1.0 fusion.2
  140.6 0.0 copy-start.2
  140.7 1.7 copy-done.2
  142.3 10.3 %collective-permute-start = (bf16[15,4096]{1,0:T(8,128)(2,1)S(1)}, bf16[15,4096]{1,0:T(8,128)(2,1)S(1)}, u32[]{:S(2)}, u32[]{:S(2)}) collective-permute-start(bf16[15,4096]{1,0:T(8,128)(2,1)S(1)} %slice.340), channel_id=1, source_target_pairs={{0,1},{1,2},{2,3},{3,4},{4,5},{5,6},{6,7},{7,8},{8,9},{9,10},{10,1... | collective-permute-start | bytes 368648 | tf_op jit(solution)/shard_map/ppermute | solution.py:19
  152.7 0.0 copy-done.4
  152.8 1.7 collective-permute-done
  154.4 2.8 %maximum_convert_fusion = f32[399,4096]{1,0:T(8,128)S(1)} fusion(bf16[384,4096]{1,0:T(8,128)(2,1)} %copy-done.2, bf16[15,4096]{1,0:T(8,128)(2,1)S(1)} %collective-permute-done), kind=kLoop, calls=%fused_computation.9 | loop fusion | flops 6537216 | bytes 9805824 | tf_op jit(solution)/shard_map/convert_element_type | solution.py:47
  157.3 3.3 %fusion.56 = bf16[384,1,1024]{2,0,1:T(8,128)(2,1)} fusion(f32[384]{0:T(512)S(1)} %fusion.57, f32[399,4096]{1,0:T(8,128)S(1)} %maximum_convert_fusion), kind=kLoop, calls=%fused_computation.112 | loop fusion | flops 7077888 | bytes 25953792 | tf_op jit(solution)/shard_map/stack | solution.py:60
  160.6 3.5 %fusion.50 = (bf16[384,1,1024]{2,0,1:T(8,128)(2,1)}, bf16[384,1,1024]{2,0,1:T(8,128)(2,1)}, bf16[384,1,1024]{2,0,1:T(8,128)(2,1)}) fusion(f32[384]{0:T(512)S(1)} %fusion.60, f32[399,4096]{1,0:T(8,128)S(1)} %maximum_convert_fusion, f32[384]{0:T(512)S(1)} %get-tuple-element.18, f32[384]{0:T(512)S(1)} %get-tuple-element.17), kind=kLoop, calls=%fused_computation.106 | loop fusion | flops 7864320 | bytes 24384000 | tf_op jit(solution)/shard_map/stack | solution.py:60
  164.1 0.0 all-gather.3.cloned.1.call-done
  164.1 7.9 %fusion.22 = f32[4,48,8,1024]{3,2,1,0:T(8,128)S(1)} fusion(bf16[4,1024,1024]{2,1,0:T(8,128)(2,1)} %all-gather.3.cloned.1.call-done, bf16[384,1,1024]{2,0,1:T(8,128)(2,1)} %fusion.56, bf16[384,1,1024]{2,0,1:T(8,128)(2,1)} %get-tuple-element.10, bf16[384,1,1024]{2,0,1:T(8,128)(2,1)} %get-tuple-element.9, bf16[384,1,1024]{2,0,1:T(8,128)(2,1)} %get-tuple-element.8), kind=kOutput, calls=%fused_computation.28 | convolution fusion | flops 3225944064 | bytes 17825792 | tf_op jit(solution)/shard_map/rgc,gcn->rgn/dot_general | solution.py:63
  172.0 0.6 copy.11
  172.6 0.0 copy-start
  172.6 1.2 multiply_reduce_fusion
  173.8 1.4 copy-done
  175.3 1.6 multiply_convert_fusion
  176.9 4.6 %collective-permute-start.1 = (bf16[15,4096]{1,0:T(8,128)(2,1)S(1)}, bf16[15,4096]{1,0:T(8,128)(2,1)S(1)}, u32[]{:S(2)}, u32[]{:S(2)}) collective-permute-start(bf16[15,4096]{1,0:T(8,128)(2,1)S(1)} %slice.371), channel_id=1, source_target_pairs={{0,1},{1,2},{2,3},{3,4},{4,5},{5,6},{6,7},{7,8},{8,9},{9,10},{10,1... | collective-permute-start | bytes 368648 | tf_op jit(solution)/shard_map/ppermute | solution.py:19
  181.5 4.6 %collective-permute-done.1 = bf16[15,4096]{1,0:T(8,128)(2,1)S(1)} collective-permute-done((bf16[15,4096]{1,0:T(8,128)(2,1)S(1)}, bf16[15,4096]{1,0:T(8,128)(2,1)S(1)}, u32[]{:S(2)}, u32[]{:S(2)}) %collective-permute-start.1) | collective-permute-done | bytes 122912 | tf_op jit(solution)/shard_map/ppermute | solution.py:19
  186.1 0.9 maximum_convert_fusion.1
  187.0 3.3 %fusion.55 = bf16[384,1,1024]{2,0,1:T(8,128)(2,1)} fusion(f32[384]{0:T(512)S(1)} %fusion.57, f32[399,4096]{1,0:T(8,128)S(1)} %maximum_convert_fusion.1), kind=kLoop, calls=%fused_computation.111 | loop fusion | flops 7077888 | bytes 25953792 | tf_op jit(solution)/shard_map/stack | solution.py:60
  190.2 3.5 %fusion.49 = (bf16[384,1,1024]{2,0,1:T(8,128)(2,1)}, bf16[384,1,1024]{2,0,1:T(8,128)(2,1)}, bf16[384,1,1024]{2,0,1:T(8,128)(2,1)}) fusion(f32[384]{0:T(512)S(1)} %fusion.60, f32[399,4096]{1,0:T(8,128)S(1)} %maximum_convert_fusion.1, f32[384]{0:T(512)S(1)} %get-tuple-element.18, f32[384]{0:T(512)S(1)} %get-tuple-element.17), kind=kLoop, calls=%fused_computation.105 | loop fusion | flops 7864320 | bytes 24384000 | tf_op jit(solution)/shard_map/stack | solution.py:60
  193.8 11.1 %all-gather.5.cloned.1.call-done = bf16[4,1024,1024]{2,1,0:T(8,128)(2,1)} async-done(((bf16[4,1024,128]{2,1,0:T(8,128)(2,1)}), bf16[4,1024,1024]{2,1,0:T(8,128)(2,1)}) %all-gather.5.cloned.1.call-update) | async-done | bytes 8388624 | tf_op jit(solution)/shard_map/all_gather | solution.py:66
  204.9 0.0 slice-start
  204.9 0.0 slice-start.1
  204.9 7.9 %fusion.19 = f32[4,48,8,1024]{3,2,1,0:T(8,128)S(1)} fusion(bf16[4,1024,1024]{2,1,0:T(8,128)(2,1)} %all-gather.5.cloned.1.call-done, bf16[384,1,1024]{2,0,1:T(8,128)(2,1)} %fusion.55, bf16[384,1,1024]{2,0,1:T(8,128)(2,1)} %get-tuple-element.7, bf16[384,1,1024]{2,0,1:T(8,128)(2,1)} %get-tuple-element.6, bf16[384,1,1024]{2,0,1:T(8,128)(2,1)} %get-tuple-element.5), kind=kOutput, calls=%fused_computation.27 | convolution fusion | flops 3225944064 | bytes 17825792 | tf_op jit(solution)/shard_map/rgc,gcn->rgn/dot_general | solution.py:63
  212.8 3.4 %copy.12 = f32[4,48,8,1024]{3,2,0,1:T(8,128)} copy(f32[4,48,8,1024]{3,2,1,0:T(8,128)S(1)} %fusion.19) | data formatting | bytes 12582912 | tf_op jit(solution)/shard_map/reshape | solution.py:69
  216.2 0.0 slice-done
  216.2 0.0 slice-done.1
  216.2 6.2 %add_convert_fusion = bf16[384,4096]{1,0:T(8,128)(2,1)} fusion(f32[384,4096]{1,0:T(8,128)} %bitcast.43, f32[4096]{0:T(1024)S(1)} %bitcast.51, f32[384,4096]{1,0:T(8,128)S(1)} %bitcast.42, f32[4096]{0:T(1024)S(1)} %bitcast.50, bf16[384,4096]{1,0:T(8,128)(2,1)S(1)} %copy-done.1), kind=kLoop, calls=%fused_computation.6 | loop fusion | flops 9437184 | bytes 18907136 | tf_op jit(solution)/shard_map/convert_element_type | solution.py:70
  (10 shorter events, 0.2 us)
Async XLA Ops:
  6.5 157.6 %all-gather.3.cloned.1.call-start = ((), (), s32[]{:S(2)}) async-start(), calls=%async_computation.2 | async-start | bytes 9437184 | tf_op jit(solution)/shard_map/all_gather | solution.py:66
  78.4 126.5 %all-gather.5.cloned.1.call-start = ((), (), s32[]{:S(2)}) async-start(), calls=%async_computation.3 | async-start | bytes 9437184 | tf_op jit(solution)/shard_map/all_gather | solution.py:66
  136.5 2.4 %copy-start.1 = (bf16[384,4096]{1,0:T(8,128)(2,1)S(1)}, bf16[384,4096]{1,0:T(8,128)(2,1)}, u32[]{:S(2)}) copy-start(bf16[384,4096]{1,0:T(8,128)(2,1)} %param.4) | copy-start | bytes 9437188
  138.8 0.8 copy-start.3
  139.6 13.1 %copy-start.4 = (f32[2,4096]{1,0:T(2,128)S(1)}, f32[2,4096]{1,0:T(2,128)}, u32[]{:S(2)}) copy-start(f32[2,4096]{1,0:T(2,128)} %param.7) | copy-start | bytes 98308
  140.6 1.7 copy-start.2
  142.3 12.1 %collective-permute-start = (bf16[15,4096]{1,0:T(8,128)(2,1)S(1)}, bf16[15,4096]{1,0:T(8,128)(2,1)S(1)}, u32[]{:S(2)}, u32[]{:S(2)}) collective-permute-start(bf16[15,4096]{1,0:T(8,128)(2,1)S(1)} %slice.340), channel_id=1, source_target_pairs={{0,1},{1,2},{2,3},{3,4},{4,5},{5,6},{6,7},{7,8},{8,9},{9,10},{10,1... | collective-permute-start | bytes 368648 | tf_op jit(solution)/shard_map/ppermute | solution.py:19
  172.6 2.7 %copy-start = (f32[4,48,8,1024]{3,2,0,1:T(8,128)}, f32[4,48,8,1024]{3,2,0,1:T(8,128)S(1)}, u32[]{:S(2)}) copy-start(f32[4,48,8,1024]{3,2,0,1:T(8,128)S(1)} %copy.11) | copy-start | bytes 18874372
  176.9 9.2 %collective-permute-start.1 = (bf16[15,4096]{1,0:T(8,128)(2,1)S(1)}, bf16[15,4096]{1,0:T(8,128)(2,1)S(1)}, u32[]{:S(2)}, u32[]{:S(2)}) collective-permute-start(bf16[15,4096]{1,0:T(8,128)(2,1)S(1)} %slice.371), channel_id=1, source_target_pairs={{0,1},{1,2},{2,3},{3,4},{4,5},{5,6},{6,7},{7,8},{8,9},{9,10},{10,1... | collective-permute-start | bytes 368648 | tf_op jit(solution)/shard_map/ppermute | solution.py:19
  204.9 11.3 %slice-start = ((s8[6291456]{0:T(1024)(128)(4,1)}), s8[4194304]{0:T(1024)(128)(4,1)S(1)}, s32[]{:S(2)}) async-start(s8[6291456]{0:T(1024)(128)(4,1)} %bitcast.40), calls=%async_computation.4 | async-start | bytes 8388608
  204.9 11.3 %slice-start.1 = ((s8[6291456]{0:T(1024)(128)(4,1)}), s8[2097152]{0:T(1024)(128)(4,1)S(1)}, s32[]{:S(2)}) async-start(s8[6291456]{0:T(1024)(128)(4,1)} %bitcast.40), calls=%async_computation.5 | async-start | bytes 4194304
Sparse Core Ops, SparseCore 0:
  78.5 62.6 all-gather.2
  143.1 61.7 all-gather.4
where the time goes:
time: 230 us; the launch traced here: 229 us
  blocking collectives  127 us (55%)
  other arithmetic  28.1 us (12%)
  waiting for transfers between devices  17.5 us (8%)
  matrix products  15.8 us (7%)
  starting transfers between devices  15 us (7%)
  between operations  13.6 us (6%)
  local copies, waits for them, and re-layouts  12.1 us (5%)
    all_to_all x2, blocking collectives, sent_to_all(): lax.all_to_all(jnp.broadcast_to(x[None], (length, *x.shape)), axis, 0, 0,...  127 us
    dot_general x2, matrix products, per_device(): jnp.einsum('rgc,gcn->rgn', pooled, lax.all_gather(full_rows, 'tp', axis=2...  15.8 us
    ppermute x2, starting transfers between devices, from_behind(): return lax.ppermute(block, axis, route)  14.9 us
    another operation x4, other arithmetic, per_device(): pooled = jnp.stack(pieces, axis=1)  13.6 us
    all_gather x2, waiting for transfers between devices, per_device(): lax.all_gather(full_rows, 'tp', axis=2, tiled=True)  11.1 us
    ppermute x2, waiting for transfers between devices, from_behind(): return lax.ppermute(block, axis, route)  6.25 us
    convert_element_type x1, other arithmetic, per_device(): return residual.astype(jnp.bfloat16)  6.2 us
  transfers between devices with their start and end apart: 4, of which 3 were waited for; matrix products, arithmetic and copies ran while one was open for 14% of the time, Pallas kernels for 0%

commit v1 on v0

v1 whole, which is shorter than its diff:
```python
import functools

import jax
import jax.numpy as jnp
from jax import lax
from jax.experimental import pallas as pl
from jax.experimental.pallas import tpu as pltpu
from jax.sharding import PartitionSpec as P

MESH = pl.DeviceIdType.MESH
F32 = jnp.float32
BF16 = jnp.bfloat16

LAYERS = 2
GROUPS = 4
SLOTS = 2
HALO = 32
EPS = 1e-06
CORES = 2
RING = 16
SIDE = 4
CW, CCW = 0, 1
SPLIT = 80
BLOCK = 112
BLOCK_SKIP = 16


def kernel(stream, mixw, gain, bscale, out, W, xs, nb, pb, res, ob, own_ss, peer_ss, scale, band,
           stage_sem, peer_sem, row_sem, prow_sem, halo_sem, ss_sem, zA, zB, xF, xL, xS, bX, bS,
           s_peer, s_prow, s_halo, s_ss, s_zA, s_xA, s_zB, s_xB, out_l, out_s, out_r):
    z = lax.axis_index("sp")
    tp = lax.axis_index("tp")
    x = tp // CORES
    core = lax.rem(tp, CORES)
    peer = 1 - core
    own_rows = stream.shape[0]
    gw = stream.shape[1] // GROUPS
    depth = mixw.shape[2]
    shard = mixw.shape[3]
    wide = CORES * shard
    rows = xs.shape[0]
    chip_rows = CORES * own_rows

    def group_of(c, s):
        return c if s == 0 else GROUPS - 1 - c

    def ring_z(d):
        return lax.rem(z + (1 if d == CW else RING - 1), RING)

    def ring_x(step):
        return lax.rem(x + step + SIDE, SIDE)

    def at_z(d):
        return {"sp": ring_z(d)}

    def at_x(step):
        return {"tp": ring_x(step) * CORES + core}

    at_peer = {"tp": x * CORES + peer}

    def source_z(d, r):
        return lax.rem(z + (RING - r if d == CW else r), RING)

    def send(src, dst, ssem, rsem, dev):
        pltpu.make_async_remote_copy(
            src_ref=src, dst_ref=dst, send_sem=ssem, recv_sem=rsem, device_id=dev, device_id_type=MESH
        ).start()

    def arrived(ref, sem):
        pltpu.make_async_copy(ref, ref, sem).wait()

    chip = z * SIDE + x
    chips = RING * SIDE
    ahead = lax.rem(chip + 1, chips)
    behind = lax.rem(chip + chips - 1, chips)
    barrier = pltpu.get_barrier_semaphore()

    def greet(dev):
        pl.semaphore_signal(barrier, inc=1, device_id=dev, device_id_type=MESH)

    for dev in (at_z(CW), at_z(CCW), at_x(1), at_x(-1), at_peer,
                {"sp": behind // SIDE, "tp": lax.rem(behind, SIDE) * CORES + CORES - 1}):
        greet(dev)

    stage = []
    for l in range(LAYERS):
        for s in range(SLOTS):
            cp = pltpu.make_async_copy(
                mixw.at[l, group_of(core, s)],
                W.at[l, x, z, pl.ds(s * depth, depth), pl.ds(pl.multiple_of(core * shard, 128), shard)],
                stage_sem.at[l, s],
            )
            cp.start()
            stage.append(cp)
    local_rows = []
    for s in range(SLOTS):
        cp = pltpu.make_async_copy(
            stream.at[:, pl.ds(pl.multiple_of(group_of(core, s) * gw, 128), gw)],
            xs.at[pl.ds(pl.multiple_of(HALO + core * own_rows, 16), own_rows), pl.ds(s * gw, gw)],
            row_sem.at[s],
        )
        cp.start()
        local_rows.append(cp)

    @pl.when(core == CORES - 1)
    def _():
        pl.semaphore_wait(barrier, 7)

    @pl.when(core != CORES - 1)
    def _():
        pl.semaphore_wait(barrier, 5)

    def peer_block(l, s):
        return W.at[l, x, z, pl.ds(s * depth, depth), pl.ds(pl.multiple_of(core * shard, 128), shard)]

    for l in range(LAYERS):
        for s in range(SLOTS):
            send(mixw.at[l, group_of(peer, s)], peer_block(l, s), s_peer.at[l, s], peer_sem.at[l, s], at_peer)

    def peer_rows(s):
        return (
            stream.at[:, pl.ds(pl.multiple_of(group_of(peer, s) * gw, 128), gw)],
            xs.at[pl.ds(pl.multiple_of(HALO + core * own_rows, 16), own_rows), pl.ds(s * gw, gw)],
        )

    for s in range(SLOTS):
        src, dst = peer_rows(s)
        send(src, dst, s_prow.at[s], prow_sem.at[s], at_peer)

    def part_a(l, xx, zz):
        return W.at[l, xx, zz, pl.ds(0, SPLIT), :]

    def part_b(l, xx, zz):
        return W.at[l, xx, zz, pl.ds(SPLIT, SLOTS * depth - SPLIT), :]

    def pair_b(l, sub, zz):
        half = x // 2 if sub == 0 else 1 - x // 2
        return W.at[l, pl.ds(2 * half, 2), zz, pl.ds(SPLIT, SLOTS * depth - SPLIT), :]

    def x_sends(l, d, r, src):
        if d == CW:
            send(src, src, s_xA.at[l], xF.at[l, CW, r], at_x(1))
            send(src, src, s_xA.at[l], xL.at[l, CW], at_x(-1))
        else:
            send(src, src, s_xA.at[l], xF.at[l, CCW, r], at_x(-1))
            send(src, src, s_xA.at[l], xL.at[l, CCW], at_x(1))

    def major(l):
        return CW if l == 0 else CCW

    def on_a(l, d, r, onward):
        src = part_a(l, x, source_z(d, r))
        arrived(src, zA.at[l, d, r - 1])
        if onward:
            send(src, src, s_zA.at[l], zA.at[l, d, r], at_z(d))
        x_sends(l, d, r, src)

    def on_xf(l, d, r):
        src = part_a(l, ring_x(-1 if d == CW else 1), source_z(d, r))
        arrived(src, xF.at[l, d, r])
        send(src, src, s_xA.at[l], xS.at[l], at_x(1 if d == CW else -1))

    def on_b(l, sub, d, r, onward):
        src = pair_b(l, sub, source_z(d, r))
        arrived(src, zB.at[l, sub, d, r - 1])
        if onward:
            send(src, src, s_zB.at[l], zB.at[l, sub, d, r], at_z(d))

    def first_a(l):
        src = part_a(l, x, z)
        for d in (CW, CCW):
            send(src, src, s_zA.at[l], zA.at[l, d, 0], at_z(d))
        x_sends(l, 1 - major(l), 0, src)

    def first_bx(l):
        src = part_b(l, x, z)
        send(src, src, s_xB.at[l], bX.at[l, CW], at_x(1))
        send(src, src, s_xB.at[l], bX.at[l, CCW], at_x(-1))

    def on_bx(l):
        from_left = part_b(l, ring_x(-1), z)
        from_right = part_b(l, ring_x(1), z)
        arrived(from_left, bX.at[l, CW])
        if l == 0:
            send(from_left, from_left, s_xB.at[l], bS.at[l], at_x(1))
        arrived(from_right, bX.at[l, CCW])
        if l == 1:
            send(from_right, from_right, s_xB.at[l], bS.at[l], at_x(-1))

    def first_b(l, sub):
        src = pair_b(l, sub, z)
        for d in (CW, CCW):
            send(src, src, s_zB.at[l], zB.at[l, sub, d, 0], at_z(d))

    def on_bs(l):
        far = part_b(l, ring_x(2), z)
        arrived(far, bS.at[l])

    for l in range(LAYERS):
        for s in range(SLOTS):
            stage[l * SLOTS + s].wait()
            got = W.at[l, x, z, pl.ds(s * depth, depth), pl.ds(pl.multiple_of(peer * shard, 128), shard)]
            arrived(got, peer_sem.at[l, s])
        if l == 0:
            first_a(0)
        first_bx(l)

    def halo_pair(c, s):
        return (
            stream.at[pl.ds(own_rows - HALO, HALO), pl.ds(group_of(c, s) * gw, gw)],
            xs.at[pl.ds(0, HALO), pl.ds(s * gw, gw)],
        )

    @pl.when(core == CORES - 1)
    def _():
        for c in range(CORES):
            for s in range(SLOTS):
                src, dst = halo_pair(c, s)
                send(src, dst, s_halo.at[c, s], halo_sem.at[s],
                     {"sp": ahead // SIDE, "tp": lax.rem(ahead, SIDE) * CORES + c})

    def window(s):
        return lax.shift_left(jnp.int32(2), group_of(core, s))

    def load_rows():
        for s in range(SLOTS):
            local_rows[s].wait()
            arrived(xs.at[pl.ds(pl.multiple_of(HALO + peer * own_rows, 16), own_rows), pl.ds(s * gw, gw)],
                    prow_sem.at[s])
            arrived(xs.at[pl.ds(0, HALO), pl.ds(s * gw, gw)], halo_sem.at[s])

        @pl.when(chip == 0)
        def _():
            xs[pl.ds(0, HALO), :] = jnp.zeros((HALO, SLOTS * gw), BF16)

    def squares():
        def body(i, carry):
            at = pl.ds(pl.multiple_of(i * 32, 32), 32)
            total = None
            for k in range(SLOTS * gw // 128):
                v = xs[at, k * 128:(k + 1) * 128].astype(F32)
                total = v * v if total is None else total + v * v
            own_ss[0, at, :] = total
            return carry

        lax.fori_loop(0, rows // 32, body, 0)

    def send_ss(l):
        send(own_ss.at[l], peer_ss.at[l], s_ss.at[l], ss_sem.at[l], at_peer)

    def scales(l):
        arrived(peer_ss.at[l], ss_sem.at[l])
        total = jnp.sum(own_ss[l] + peer_ss[l], axis=1, keepdims=True)
        s = lax.rsqrt(total / float(GROUPS * gw) + EPS)
        scale[...] = jnp.broadcast_to(s, (rows, 128))

    def normalize(l):
        src = xs if l == 0 else res
        gains = [gain[l:l + 1, pl.ds(pl.multiple_of(group_of(core, s) * gw, 128), gw)] for s in range(SLOTS)]

        def body(i, carry):
            at = pl.ds(pl.multiple_of(i * 32, 32), 32)
            sc = scale[at, :]
            for s in range(SLOTS):
                for k in range(gw // 128):
                    col = slice(s * gw + k * 128, s * gw + (k + 1) * 128)
                    v = src[at, col].astype(F32)
                    nb[at, col] = (v * sc * gains[s][:, k * 128:(k + 1) * 128]).astype(BF16)
            return carry

        lax.fori_loop(0, rows // 32, body, 0)

    first_row = chip * chip_rows - HALO

    def pool(i):
        base = i * BLOCK
        above = pl.ds(pl.multiple_of(base, 16), BLOCK + BLOCK_SKIP)
        here = pl.ds(pl.multiple_of(base + BLOCK_SKIP, 16), BLOCK)
        to = pl.ds(pl.multiple_of(base, 16), BLOCK)
        count = first_row + base + BLOCK_SKIP + 1 + lax.broadcasted_iota(jnp.int32, (BLOCK, 128), 0)
        for s in range(SLOTS):
            inverse = 1.0 / jnp.maximum(jnp.minimum(count, window(s)), 1).astype(F32)
            for k in range(gw // 256):
                cols = slice(s * gw + k * 256, s * gw + (k + 1) * 256)
                total = jnp.dot(band[s], nb[above, cols], preferred_element_type=F32)
                for h in range(2):
                    col = slice(s * gw + k * 256 + h * 128, s * gw + k * 256 + (h + 1) * 128)
                    mean = total[:, h * 128:(h + 1) * 128] * inverse
                    pb[to, col] = (mean - nb[here, col].astype(F32)).astype(BF16)

    def mix(l, s, xx):
        lhs = pb[:, pl.ds(pl.multiple_of(s * gw, 128), gw)]
        w = W[l, xx, :, pl.ds(pl.multiple_of(s * depth, 16), depth), :].reshape(RING * depth, wide)
        total = jnp.dot(lhs, w, preferred_element_type=F32)
        g = jnp.where(s == 0, core, GROUPS - 1 - core)
        gcol = pl.ds(pl.multiple_of(g * gw + xx * wide, 128), wide)
        col = pl.ds(pl.multiple_of(s * gw + xx * wide, 128), wide)
        by = bscale[l:l + 1, gcol]
        if l == 0:
            r = xs[BLOCK_SKIP:, col].astype(F32) + total * by
            res[BLOCK_SKIP:, col] = r
            own_ss[1, BLOCK_SKIP:, :] += r[:, :128] * r[:, :128] + r[:, 128:] * r[:, 128:]
        else:
            r = res[HALO:, col] + total[HALO - BLOCK_SKIP:] * by
            p = s * SIDE + xx
            ob[p] = r.astype(BF16)
            mine = pl.ds(pl.multiple_of(core * own_rows, 16), own_rows)
            theirs = pl.ds(pl.multiple_of(peer * own_rows, 16), own_rows)
            send(ob.at[p, theirs], out.at[:, gcol], out_s, out_r, at_peer)
            pltpu.make_async_copy(ob.at[p, mine], out.at[:, gcol], out_l).start()

    for s in range(SLOTS):
        gap = BLOCK_SKIP + lax.broadcasted_iota(jnp.int32, (BLOCK, BLOCK + BLOCK_SKIP), 0) - lax.broadcasted_iota(
            jnp.int32, (BLOCK, BLOCK + BLOCK_SKIP), 1)
        band[s] = jnp.where((gap >= 0) & (gap < window(s)), 1.0, 0.0).astype(BF16)
    own_ss[1] = jnp.zeros((rows, 128), F32)
    res[:BLOCK_SKIP, :] = jnp.zeros((BLOCK_SKIP, SLOTS * gw), F32)

    on_bx(0)
    first_b(0, 0)
    load_rows()
    squares()
    send_ss(0)
    on_bs(0)
    first_b(0, 1)
    on_bx(1)

    last = RING // 2

    def body0(r, carry):
        on_a(0, CW, r, True)
        on_a(0, CCW, r, True)
        on_xf(0, CCW, r - 1)

        @pl.when(r > 1)
        def _():
            on_xf(0, CW, r - 1)

        @pl.when(r == 1)
        def _():
            scales(0)
            normalize(0)

        on_b(0, 0, CW, r, True)
        on_b(0, 0, CCW, r, True)
        pool(r - 1)
        on_b(0, 1, CW, r, True)
        on_b(0, 1, CCW, r, True)
        return carry

    lax.fori_loop(1, last - 1, body0, 0)
    r = last - 1
    on_a(0, CW, r, True)
    on_a(0, CCW, r, False)
    on_xf(0, CCW, r - 1)
    on_xf(0, CW, r - 1)
    on_bs(1)
    on_b(0, 0, CW, r, True)
    on_b(0, 0, CCW, r, False)
    first_a(1)
    pool(r - 1)
    on_b(0, 1, CW, r, False)
    on_b(0, 1, CCW, r, True)
    first_b(1, 0)
    first_b(1, 1)
    r = last
    on_a(0, CW, r, False)
    on_xf(0, CCW, r - 1)
    on_xf(0, CW, r - 1)
    on_b(0, 0, CW, r, False)
    on_b(0, 1, CCW, r, False)

    def finish_gather0():
        arrived(W.at[0, ring_x(1), pl.ds(0, last), pl.ds(0, SPLIT), :], xL.at[0, CW])
        arrived(W.at[0, ring_x(-1), pl.ds(0, last), pl.ds(0, SPLIT), :], xL.at[0, CCW])
        arrived(W.at[0, ring_x(2), :, pl.ds(0, SPLIT), :], xS.at[0])

    def filler(r, spot):
        q = (r - 2) * 3 + spot

        @pl.when((q >= 0) & (q < SLOTS * SIDE))
        def _():
            mix(0, q // SIDE, lax.rem(q, SIDE))

        if spot == 2:
            @pl.when(r == 4)
            def _():
                send_ss(1)

        if spot == 0:
            @pl.when(r == 5)
            def _():
                scales(1)
                normalize(1)

        i = (r - 5) * 3 + spot - 1

        @pl.when((i >= 0) & (i < rows // BLOCK))
        def _():
            pool(i)

    def body1(r, carry):
        on_a(1, CW, r, True)
        on_a(1, CCW, r, True)
        on_xf(1, CW, r - 1)

        @pl.when(r > 1)
        def _():
            on_xf(1, CCW, r - 1)

        @pl.when(r == 1)
        def _():
            on_xf(0, CW, last)

        @pl.when(r == 2)
        def _():
            finish_gather0()

        filler(r, 0)
        on_b(1, 0, CW, r, True)
        on_b(1, 0, CCW, r, True)
        filler(r, 1)
        on_b(1, 1, CW, r, True)
        on_b(1, 1, CCW, r, True)
        filler(r, 2)
        return carry

    lax.fori_loop(1, last - 1, body1, 0)
    r = last - 1
    on_a(1, CW, r, False)
    on_a(1, CCW, r, True)
    on_xf(1, CW, r - 1)
    on_xf(1, CCW, r - 1)
    on_b(1, 0, CW, r, True)
    on_b(1, 0, CCW, r, False)
    pool(5)
    on_b(1, 1, CW, r, False)
    on_b(1, 1, CCW, r, True)
    pool(6)
    r = last
    on_a(1, CCW, r, False)
    on_xf(1, CW, r - 1)
    on_xf(1, CCW, r - 1)
    on_b(1, 0, CW, r, False)
    on_b(1, 1, CCW, r, False)

    def both(xx):
        def body(s, carry):
            mix(1, s, xx)
            return carry

        lax.fori_loop(0, SLOTS, body, 0)

    def tail(j, carry):
        @pl.when(j == 1)
        def _():
            on_xf(1, CCW, last)
            arrived(W.at[1, ring_x(-1), pl.ds(0, last), pl.ds(0, SPLIT), :], xL.at[1, CCW])
            arrived(W.at[1, ring_x(1), pl.ds(0, last), pl.ds(0, SPLIT), :], xL.at[1, CW])

        @pl.when(j == 3)
        def _():
            arrived(W.at[1, ring_x(2), :, pl.ds(0, SPLIT), :], xS.at[1])

        step = jnp.where(j == 2, 3, jnp.where(j == 3, 2, j))
        both(lax.rem(x + step, SIDE))
        return carry

    lax.fori_loop(0, SIDE, tail, 0)

    for l in range(LAYERS):
        arrived(W.at[l, 0, pl.ds(0, RING - 1), pl.ds(0, SPLIT), :], s_zA.at[l])
        arrived(W.at[l, pl.ds(0, SIDE - 1), :, pl.ds(0, SPLIT), :], s_xA.at[l])
        arrived(W.at[l, pl.ds(0, SIDE - 1), 0, pl.ds(SPLIT, SLOTS * depth - SPLIT), :], s_xB.at[l])
        arrived(W.at[l, :, pl.ds(0, RING - 1), pl.ds(SPLIT, SLOTS * depth - SPLIT), :], s_zB.at[l])
        arrived(own_ss.at[l], s_ss.at[l])
        for s in range(SLOTS):
            arrived(peer_block(l, s), s_peer.at[l, s])
    for s in range(SLOTS):
        arrived(peer_rows(s)[1], s_prow.at[s])

    @pl.when(core == CORES - 1)
    def _():
        for c in range(CORES):
            for s in range(SLOTS):
                arrived(halo_pair(c, s)[1], s_halo.at[c, s])

    for sem in (out_s, out_r, out_l):
        arrived(ob.at[:, pl.ds(0, own_rows), :], sem)


def per_device(stream, norm_gain, mix_weight, branch_scale):
    own_rows, width = stream.shape
    depth, shard = mix_weight.shape[2:]
    rows = HALO + CORES * own_rows
    half = SLOTS * width // GROUPS
    wide = CORES * shard
    dma = pltpu.SemaphoreType.DMA
    last = RING // 2
    any_space = pl.BlockSpec(memory_space=pl.ANY)
    vmem = pl.BlockSpec(memory_space=pltpu.VMEM)
    return pl.pallas_call(
        kernel,
        out_shape=jax.ShapeDtypeStruct((own_rows, width), BF16),
        in_specs=[any_space, any_space, vmem, vmem],
        out_specs=any_space,
        scratch_shapes=[
            pltpu.VMEM((LAYERS, SIDE, RING, SLOTS * depth, wide), BF16),
            pltpu.VMEM((rows, half), BF16),
            pltpu.VMEM((rows, half), BF16),
            pltpu.VMEM((rows - BLOCK_SKIP, half), BF16),
            pltpu.VMEM((rows, half), F32),
            pltpu.VMEM((SLOTS * SIDE, CORES * own_rows, wide), BF16),
            pltpu.VMEM((LAYERS, rows, 128), F32),
            pltpu.VMEM((LAYERS, rows, 128), F32),
            pltpu.VMEM((rows, 128), F32),
            pltpu.VMEM((SLOTS, BLOCK, BLOCK + BLOCK_SKIP), BF16),
            dma((LAYERS, SLOTS)),
            dma((LAYERS, SLOTS)),
            dma((SLOTS,)),
            dma((SLOTS,)),
            dma((SLOTS,)),
            dma((LAYERS,)),
            dma((LAYERS, 2, last)),
            dma((LAYERS, 2, 2, last)),
            dma((LAYERS, 2, last + 1)),
            dma((LAYERS, 2)),
            dma((LAYERS,)),
            dma((LAYERS, 2)),
            dma((LAYERS,)),
            dma((LAYERS, SLOTS)),
            dma((SLOTS,)),
            dma((CORES, SLOTS)),
            dma((LAYERS,)),
            dma((LAYERS,)),
            dma((LAYERS,)),
            dma((LAYERS,)),
            dma((LAYERS,)),
            dma(()),
            dma(()),
            dma(()),
        ],
        compiler_params=pltpu.CompilerParams(
            collective_id=0, has_side_effects=True, vmem_limit_bytes=60 * 1024 * 1024
        ),
        cost_estimate=pl.CostEstimate(flops=7 * 10**9, bytes_accessed=10**7, transcendentals=0),
    )(stream, mix_weight, norm_gain, branch_scale)


def solution(mesh):
    assert mesh.shape["sp"] == RING and mesh.shape["tp"] == SIDE * CORES
    return jax.shard_map(
        per_device,
        mesh=mesh,
        in_specs=(P(("grp", "sp", "tp"), None), P(), P(None, None, "sp", "tp"), P()),
        out_specs=P(("grp", "sp", "tp"), None),
        check_vma=False,
    )
```

time: 230 us -> 105 us (0.46)
  blocking collectives: 127 us -> 0 us
  Pallas kernels: 0 us -> 101 us
  other arithmetic: 28.1 us -> 0 us
  waiting for transfers between devices: 17.5 us -> 0 us
  matrix products: 15.8 us -> 0 us
  starting transfers between devices: 15 us -> 0 us
  between operations: 13.6 us -> 0.01 us
  local copies, waits for them, and re-layouts: 12.1 us -> 3.91 us
    all_to_all x2 -> x0, blocking collectives: 127 us -> none  [sent_to_all(): lax.all_to_all(jnp.broadcast_to(x[None], (length, *x.shape)), axis, 0, 0,...]
    pallas_call x0 -> x1, Pallas kernels: none -> 101 us  [per_device(): pl.pallas_call(kernel, out_shape=jax.ShapeDtypeStruct((own_rows, width),...]
    dot_general x2 -> x0, matrix products: 15.8 us -> none  [per_device(): jnp.einsum('rgc,gcn->rgn', pooled, lax.all_gather(full_rows, 'tp', axis=2...]
    ppermute x2 -> x0, starting transfers between devices: 14.9 us -> none  [from_behind(): return lax.ppermute(block, axis, route)]
    another operation x4 -> x0, other arithmetic: 13.6 us -> none  [per_device(): pooled = jnp.stack(pieces, axis=1)]
    convert_element_type x5 -> x0, other arithmetic: 12.5 us -> none  [the longest x1 6.2 us: per_device(): return residual.astype(jnp.bfloat16)]
    all_gather x2 -> x0, waiting for transfers between devices: 11.1 us -> none  [per_device(): lax.all_gather(full_rows, 'tp', axis=2, tiled=True)]
    ppermute x2 -> x0, waiting for transfers between devices: 6.25 us -> none  [from_behind(): return lax.ppermute(block, axis, route)]
  transfers between devices with their start and end apart: 4 -> 0, of which waited for: 3 -> 0; matrix products, arithmetic and copies ran while one was open for 14% -> 0% of each run, Pallas kernels for 0% -> 0%
where the time goes in v1:
time: 105 us
  Pallas kernels  101 us (96%)
  local copies, waits for them, and re-layouts  3.91 us (4%)
    pallas_call x1, Pallas kernels, per_device(): pl.pallas_call(kernel, out_shape=jax.ShapeDtypeStruct((own_rows, width),...  101 us
    unnamed x1, local copies, waits for them, and re-layouts  3.91 us

profile of v1, /device:TPU:33, one launch (start us, length us, event | category | flops | bytes accessed | tf_op | source)
XLA Modules:
  0.0 104.9 jit_solution(16783724138560727024)
XLA Ops:
  0.0 101.0 %shard_map.46 = bf16[384,4096]{1,0:T(8,128)(2,1)} custom-call(bf16[384,4096]{1,0:T(8,128)(2,1)} %stream.1, bf16[2,4,64,128]{3,2,1,0:T(8,128)(2,1)} %mixw.1, f32[2,4096]{1,0:T(2,128)} %gain.1, f32[2,4096]{1,0:T(2,128)} %bscale.1), custom_call_target="tpu_custom_call" | custom-call | flops 7000000000 | bytes 10000000 | tf_op jit(solution)/shard_map/pallas_call | solution.py:502
  101.0 3.9 %copy.6 = bf16[384,4096]{1,0:T(8,128)(2,1)} copy(bf16[384,4096]{1,0:T(8,128)(2,1)} %shard_map.46) | data formatting | bytes 6291456

commit v2 on v1

--- a/solution.py
+++ b/solution.py
@@ -20,14 +20,15 @@
 RING = 16
 SIDE = 4
 CW, CCW = 0, 1
+OFFSET = 4
 SPLIT = 80
 BLOCK = 112
 BLOCK_SKIP = 16
 
 
-def kernel(stream, mixw, gain, bscale, out, W, xs, nb, pb, res, ob, own_ss, peer_ss, scale, band,
-           stage_sem, peer_sem, row_sem, prow_sem, halo_sem, ss_sem, zA, zB, xF, xL, xS, bX, bS,
-           s_peer, s_prow, s_halo, s_ss, s_zA, s_xA, s_zB, s_xB, out_l, out_s, out_r):
+def kernel(stream, mixw, gain_hbm, bscale_hbm, out, gain, bscale, W, xs, wst, rst, nb, pb, res, ob, own_ss, peer_ss, scale, band,
+           vec_sem, stage_sem, wst_sem, rst_sem, peer_sem, row_sem, prow_sem, halo_sem, ss_sem, zA, zB, xF, xL, xS, bX, bS,
+           s_peer, s_prow, s_halo, s_ss, s_zA, s_xA, s_zB, s_xB, out_s, out_r):
     z = lax.axis_index("sp")
     tp = lax.axis_index("tp")
     x = tp // CORES
@@ -82,7 +83,7 @@
                 {"sp": behind // SIDE, "tp": lax.rem(behind, SIDE) * CORES + CORES - 1}):
         greet(dev)
 
-    stage = []
+    stage, peer_stage = [], []
     for l in range(LAYERS):
         for s in range(SLOTS):
             cp = pltpu.make_async_copy(
@@ -92,7 +93,10 @@
             )
             cp.start()
             stage.append(cp)
-    local_rows = []
+            cp = pltpu.make_async_copy(mixw.at[l, group_of(peer, s)], wst.at[l, s], wst_sem.at[l, s])
+            cp.start()
+            peer_stage.append(cp)
+    local_rows, peer_cols = [], []
     for s in range(SLOTS):
         cp = pltpu.make_async_copy(
             stream.at[:, pl.ds(pl.multiple_of(group_of(core, s) * gw, 128), gw)],
@@ -101,6 +105,17 @@
         )
         cp.start()
         local_rows.append(cp)
+        cp = pltpu.make_async_copy(
+            stream.at[:, pl.ds(pl.multiple_of(group_of(peer, s) * gw, 128), gw)],
+            rst.at[:, pl.ds(s * gw, gw)],
+            rst_sem.at[s],
+        )
+        cp.start()
+        peer_cols.append(cp)
+
+    vectors = [pltpu.make_async_copy(gain_hbm, gain, vec_sem.at[0]), pltpu.make_async_copy(bscale_hbm, bscale, vec_sem.at[1])]
+    for cp in vectors:
+        cp.start()
 
     @pl.when(core == CORES - 1)
     def _():
@@ -115,17 +130,14 @@
 
     for l in range(LAYERS):
         for s in range(SLOTS):
-            send(mixw.at[l, group_of(peer, s)], peer_block(l, s), s_peer.at[l, s], peer_sem.at[l, s], at_peer)
+            peer_stage[l * SLOTS + s].wait()
+            send(wst.at[l, s], peer_block(l, s), s_peer.at[l, s], peer_sem.at[l, s], at_peer)
 
     def peer_rows(s):
         return (
-            stream.at[:, pl.ds(pl.multiple_of(group_of(peer, s) * gw, 128), gw)],
+            rst.at[:, pl.ds(s * gw, gw)],
             xs.at[pl.ds(pl.multiple_of(HALO + core * own_rows, 16), own_rows), pl.ds(s * gw, gw)],
         )
-
-    for s in range(SLOTS):
-        src, dst = peer_rows(s)
-        send(src, dst, s_prow.at[s], prow_sem.at[s], at_peer)
 
     def part_a(l, xx, zz):
         return W.at[l, xx, zz, pl.ds(0, SPLIT), :]
@@ -148,23 +160,42 @@
     def major(l):
         return CW if l == 0 else CCW
 
-    def on_a(l, d, r, onward):
-        src = part_a(l, x, source_z(d, r))
-        arrived(src, zA.at[l, d, r - 1])
-        if onward:
-            send(src, src, s_zA.at[l], zA.at[l, d, r], at_z(d))
-        x_sends(l, d, r, src)
+    last = RING // 2
+
+    def on_a(l, d, r):
+        end = last if d == major(l) else last - 1
+
+        @pl.when((r >= 1) & (r <= end))
+        def _():
+            src = part_a(l, x, source_z(d, r))
+            arrived(src, zA.at[l, d, r - 1])
+
+            @pl.when(r < end)
+            def _():
+                send(src, src, s_zA.at[l], zA.at[l, d, r], at_z(d))
+
+            x_sends(l, d, r, src)
 
     def on_xf(l, d, r):
-        src = part_a(l, ring_x(-1 if d == CW else 1), source_z(d, r))
-        arrived(src, xF.at[l, d, r])
-        send(src, src, s_xA.at[l], xS.at[l], at_x(1 if d == CW else -1))
-
-    def on_b(l, sub, d, r, onward):
-        src = pair_b(l, sub, source_z(d, r))
-        arrived(src, zB.at[l, sub, d, r - 1])
-        if onward:
-            send(src, src, s_zB.at[l], zB.at[l, sub, d, r], at_z(d))
+        first = 1 if d == major(l) else 0
+
+        @pl.when((r >= first) & (r < first + last))
+        def _():
+            src = part_a(l, ring_x(-1 if d == CW else 1), source_z(d, r))
+            arrived(src, xF.at[l, d, r])
+            send(src, src, s_xA.at[l], xS.at[l], at_x(1 if d == CW else -1))
+
+    def on_b(l, sub, d, r):
+        end = last if d == sub else last - 1
+
+        @pl.when((r >= 1) & (r <= end))
+        def _():
+            src = pair_b(l, sub, source_z(d, r))
+            arrived(src, zB.at[l, sub, d, r - 1])
+
+            @pl.when(r < end)
+            def _():
+                send(src, src, s_zB.at[l], zB.at[l, sub, d, r], at_z(d))
 
     def first_a(l):
         src = part_a(l, x, z)
@@ -201,15 +232,21 @@
             stage[l * SLOTS + s].wait()
             got = W.at[l, x, z, pl.ds(s * depth, depth), pl.ds(pl.multiple_of(peer * shard, 128), shard)]
             arrived(got, peer_sem.at[l, s])
+        first_bx(l)
         if l == 0:
             first_a(0)
-        first_bx(l)
+
+    for s in range(SLOTS):
+        peer_cols[s].wait()
+        src, dst = peer_rows(s)
+        send(src, dst, s_prow.at[s], prow_sem.at[s], at_peer)
+        local_rows[s].wait()
 
     def halo_pair(c, s):
-        return (
-            stream.at[pl.ds(own_rows - HALO, HALO), pl.ds(group_of(c, s) * gw, gw)],
-            xs.at[pl.ds(0, HALO), pl.ds(s * gw, gw)],
-        )
+        cols = pl.ds(s * gw, gw)
+        src = xs.at[pl.ds(HALO + CORES * own_rows - HALO, HALO), cols] if c == CORES - 1 else rst.at[
+            pl.ds(own_rows - HALO, HALO), cols]
+        return src, xs.at[pl.ds(0, HALO), cols]
 
     @pl.when(core == CORES - 1)
     def _():
@@ -223,8 +260,9 @@
         return lax.shift_left(jnp.int32(2), group_of(core, s))
 
     def load_rows():
+        for cp in vectors:
+            cp.wait()
         for s in range(SLOTS):
-            local_rows[s].wait()
             arrived(xs.at[pl.ds(pl.multiple_of(HALO + peer * own_rows, 16), own_rows), pl.ds(s * gw, gw)],
                     prow_sem.at[s])
             arrived(xs.at[pl.ds(0, HALO), pl.ds(s * gw, gw)], halo_sem.at[s])
@@ -303,11 +341,20 @@
         else:
             r = res[HALO:, col] + total[HALO - BLOCK_SKIP:] * by
             p = s * SIDE + xx
-            ob[p] = r.astype(BF16)
-            mine = pl.ds(pl.multiple_of(core * own_rows, 16), own_rows)
-            theirs = pl.ds(pl.multiple_of(peer * own_rows, 16), own_rows)
-            send(ob.at[p, theirs], out.at[:, gcol], out_s, out_r, at_peer)
-            pltpu.make_async_copy(ob.at[p, mine], out.at[:, gcol], out_l).start()
+
+            def share(mine, theirs):
+                out[:, gcol] = r[mine].astype(BF16)
+                ob[p] = r[theirs].astype(BF16)
+
+            @pl.when(core == 0)
+            def _():
+                share(slice(0, own_rows), slice(own_rows, None))
+
+            @pl.when(core != 0)
+            def _():
+                share(slice(own_rows, None), slice(0, own_rows))
+
+            send(ob.at[p], out.at[:, gcol], out_s, out_r, at_peer)
 
     for s in range(SLOTS):
         gap = BLOCK_SKIP + lax.broadcasted_iota(jnp.int32, (BLOCK, BLOCK + BLOCK_SKIP), 0) - lax.broadcasted_iota(
@@ -316,157 +363,125 @@
     own_ss[1] = jnp.zeros((rows, 128), F32)
     res[:BLOCK_SKIP, :] = jnp.zeros((BLOCK_SKIP, SLOTS * gw), F32)
 
-    on_bx(0)
-    first_b(0, 0)
-    load_rows()
-    squares()
-    send_ss(0)
-    on_bs(0)
-    first_b(0, 1)
-    on_bx(1)
-
-    last = RING // 2
-
-    def body0(r, carry):
-        on_a(0, CW, r, True)
-        on_a(0, CCW, r, True)
-        on_xf(0, CCW, r - 1)
-
-        @pl.when(r > 1)
-        def _():
-            on_xf(0, CW, r - 1)
-
-        @pl.when(r == 1)
-        def _():
-            scales(0)
-            normalize(0)
-
-        on_b(0, 0, CW, r, True)
-        on_b(0, 0, CCW, r, True)
-        pool(r - 1)
-        on_b(0, 1, CW, r, True)
-        on_b(0, 1, CCW, r, True)
-        return carry
-
-    lax.fori_loop(1, last - 1, body0, 0)
-    r = last - 1
-    on_a(0, CW, r, True)
-    on_a(0, CCW, r, False)
-    on_xf(0, CCW, r - 1)
-    on_xf(0, CW, r - 1)
-    on_bs(1)
-    on_b(0, 0, CW, r, True)
-    on_b(0, 0, CCW, r, False)
-    first_a(1)
-    pool(r - 1)
-    on_b(0, 1, CW, r, False)
-    on_b(0, 1, CCW, r, True)
-    first_b(1, 0)
-    first_b(1, 1)
-    r = last
-    on_a(0, CW, r, False)
-    on_xf(0, CCW, r - 1)
-    on_xf(0, CW, r - 1)
-    on_b(0, 0, CW, r, False)
-    on_b(0, 1, CCW, r, False)
-
-    def finish_gather0():
-        arrived(W.at[0, ring_x(1), pl.ds(0, last), pl.ds(0, SPLIT), :], xL.at[0, CW])
-        arrived(W.at[0, ring_x(-1), pl.ds(0, last), pl.ds(0, SPLIT), :], xL.at[0, CCW])
-        arrived(W.at[0, ring_x(2), :, pl.ds(0, SPLIT), :], xS.at[0])
-
-    def filler(r, spot):
-        q = (r - 2) * 3 + spot
-
-        @pl.when((q >= 0) & (q < SLOTS * SIDE))
-        def _():
-            mix(0, q // SIDE, lax.rem(q, SIDE))
+    def finish_gather(l, hop):
+        if hop == 1:
+            arrived(W.at[l, ring_x(1), pl.ds(0, last), pl.ds(0, SPLIT), :], xL.at[l, CW])
+            arrived(W.at[l, ring_x(-1), pl.ds(0, last), pl.ds(0, SPLIT), :], xL.at[l, CCW])
+        else:
+            arrived(W.at[l, ring_x(2), :, pl.ds(0, SPLIT), :], xS.at[l])
+
+    def mix_many(l, start, stop):
+        def body(q, carry):
+            k = q // SLOTS
+            flip = jnp.where(k == 2, 3, jnp.where(k == 3, 2, k))
+            mix(l, lax.rem(q, SLOTS), lax.bitwise_xor(x, flip))
+            return carry
+
+        lax.fori_loop(start, stop, body, 0)
+
+    def pool_many(start, stop):
+        def body(i, carry):
+            pool(i)
+            return carry
+
+        lax.fori_loop(start, stop, body, 0)
+
+    full = 2 + last
+
+    def filler(g, spot):
+        if spot == 0:
+            @pl.when(g == 2)
+            def _():
+                load_rows()
+                squares()
+                send_ss(0)
+
+            @pl.when(g == 3)
+            def _():
+                scales(0)
+                normalize(0)
 
         if spot == 2:
-            @pl.when(r == 4)
-            def _():
-                send_ss(1)
-
-        if spot == 0:
-            @pl.when(r == 5)
+            @pl.when(g == full + 1)
             def _():
                 scales(1)
                 normalize(1)
 
-        i = (r - 5) * 3 + spot - 1
-
-        @pl.when((i >= 0) & (i < rows // BLOCK))
-        def _():
-            pool(i)
-
-    def body1(r, carry):
-        on_a(1, CW, r, True)
-        on_a(1, CCW, r, True)
-        on_xf(1, CW, r - 1)
-
-        @pl.when(r > 1)
-        def _():
-            on_xf(1, CCW, r - 1)
-
-        @pl.when(r == 1)
-        def _():
-            on_xf(0, CW, last)
-
-        @pl.when(r == 2)
-        def _():
-            finish_gather0()
-
-        filler(r, 0)
-        on_b(1, 0, CW, r, True)
-        on_b(1, 0, CCW, r, True)
-        filler(r, 1)
-        on_b(1, 1, CW, r, True)
-        on_b(1, 1, CCW, r, True)
-        filler(r, 2)
+        e = (g - full - 2) * 3 + spot
+        start = 2 * jnp.where(g <= full, (g - 4) if spot == 1 else -1, e)
+        start = jnp.where(start < 0, rows // BLOCK, start)
+        pool_many(start, jnp.minimum(start + 2, rows // BLOCK))
+
+        for l in range(LAYERS):
+            done = full + l * OFFSET
+            if spot == 2:
+                @pl.when(g == done - 1)
+                def _(l=l):
+                    mix_many(l, 0, SLOTS)
+
+                @pl.when(g == done)
+                def _(l=l):
+                    mix_many(l, 2 * SLOTS, 3 * SLOTS)
+                    finish_gather(l, 2)
+                    mix_many(l, 3 * SLOTS, 4 * SLOTS)
+                    if l == 0:
+                        send_ss(1)
+
+            if spot == 0:
+                @pl.when(g == done)
+                def _(l=l):
+                    finish_gather(l, 1)
+                    mix_many(l, SLOTS, 2 * SLOTS)
+
+    def step(g, carry):
+        for l in range(LAYERS):
+            for d in (CW, CCW):
+                on_a(l, d, g - l * OFFSET)
+
+        @pl.when(g == OFFSET)
+        def _():
+            first_a(1)
+
+        @pl.when(g == 1)
+        def _():
+            on_bx(0)
+            first_b(0, 0)
+
+        filler(g, 0)
+        for l in range(LAYERS):
+            for d in (CW, CCW):
+                on_b(l, 0, d, g - l * OFFSET - 1)
+        for l in range(LAYERS):
+            for d in (CW, CCW):
+                on_xf(l, d, g - l * OFFSET - 1)
+
+        @pl.when(g == 2)
+        def _():
+            on_bs(0)
+            first_b(0, 1)
+
+        @pl.when(g == 3)
+        def _():
+            on_bx(1)
+
+        @pl.when(g == OFFSET + 1)
+        def _():
+            first_b(1, 0)
+
+        filler(g, 1)
+        for l in range(LAYERS):
+            for d in (CW, CCW):
+                on_b(l, 1, d, g - l * OFFSET - 2)
+
+        @pl.when(g == OFFSET + 2)
+        def _():
+            on_bs(1)
+            first_b(1, 1)
+
+        filler(g, 2)
         return carry
 
-    lax.fori_loop(1, last - 1, body1, 0)
-    r = last - 1
-    on_a(1, CW, r, False)
-    on_a(1, CCW, r, True)
-    on_xf(1, CW, r - 1)
-    on_xf(1, CCW, r - 1)
-    on_b(1, 0, CW, r, True)
-    on_b(1, 0, CCW, r, False)
-    pool(5)
-    on_b(1, 1, CW, r, False)
-    on_b(1, 1, CCW, r, True)
-    pool(6)
-    r = last
-    on_a(1, CCW, r, False)
-    on_xf(1, CW, r - 1)
-    on_xf(1, CCW, r - 1)
-    on_b(1, 0, CW, r, False)
-    on_b(1, 1, CCW, r, False)
-
-    def both(xx):
-        def body(s, carry):
-            mix(1, s, xx)
-            return carry
-
-        lax.fori_loop(0, SLOTS, body, 0)
-
-    def tail(j, carry):
-        @pl.when(j == 1)
-        def _():
-            on_xf(1, CCW, last)
-            arrived(W.at[1, ring_x(-1), pl.ds(0, last), pl.ds(0, SPLIT), :], xL.at[1, CCW])
-            arrived(W.at[1, ring_x(1), pl.ds(0, last), pl.ds(0, SPLIT), :], xL.at[1, CW])
-
-        @pl.when(j == 3)
-        def _():
-            arrived(W.at[1, ring_x(2), :, pl.ds(0, SPLIT), :], xS.at[1])
-
-        step = jnp.where(j == 2, 3, jnp.where(j == 3, 2, j))
-        both(lax.rem(x + step, SIDE))
-        return carry
-
-    lax.fori_loop(0, SIDE, tail, 0)
+    lax.fori_loop(1, OFFSET + full + 1, step, 0)
 
     for l in range(LAYERS):
         arrived(W.at[l, 0, pl.ds(0, RING - 1), pl.ds(0, SPLIT), :], s_zA.at[l])
@@ -485,8 +500,8 @@
             for s in range(SLOTS):
                 arrived(halo_pair(c, s)[1], s_halo.at[c, s])
 
-    for sem in (out_s, out_r, out_l):
-        arrived(ob.at[:, pl.ds(0, own_rows), :], sem)
+    for sem in (out_s, out_r):
+        arrived(ob, sem)
 
 
 def per_device(stream, norm_gain, mix_weight, branch_scale):
@@ -497,25 +512,32 @@
     wide = CORES * shard
     dma = pltpu.SemaphoreType.DMA
     last = RING // 2
-    any_space = pl.BlockSpec(memory_space=pl.ANY)
+    hbm = pl.BlockSpec(memory_space=pltpu.HBM)
     vmem = pl.BlockSpec(memory_space=pltpu.VMEM)
     return pl.pallas_call(
         kernel,
         out_shape=jax.ShapeDtypeStruct((own_rows, width), BF16),
-        in_specs=[any_space, any_space, vmem, vmem],
-        out_specs=any_space,
+        in_specs=[hbm] * 4,
+        out_specs=vmem,
         scratch_shapes=[
+            pltpu.VMEM(norm_gain.shape, F32),
+            pltpu.VMEM(branch_scale.shape, F32),
             pltpu.VMEM((LAYERS, SIDE, RING, SLOTS * depth, wide), BF16),
             pltpu.VMEM((rows, half), BF16),
+            pltpu.VMEM((LAYERS, SLOTS, depth, shard), BF16),
+            pltpu.VMEM((own_rows, half), BF16),
             pltpu.VMEM((rows, half), BF16),
             pltpu.VMEM((rows - BLOCK_SKIP, half), BF16),
             pltpu.VMEM((rows, half), F32),
-            pltpu.VMEM((SLOTS * SIDE, CORES * own_rows, wide), BF16),
+            pltpu.VMEM((SLOTS * SIDE, own_rows, wide), BF16),
             pltpu.VMEM((LAYERS, rows, 128), F32),
             pltpu.VMEM((LAYERS, rows, 128), F32),
             pltpu.VMEM((rows, 128), F32),
             pltpu.VMEM((SLOTS, BLOCK, BLOCK + BLOCK_SKIP), BF16),
+            dma((2,)),
             dma((LAYERS, SLOTS)),
+            dma((LAYERS, SLOTS)),
+            dma((SLOTS,)),
             dma((LAYERS, SLOTS)),
             dma((SLOTS,)),
             dma((SLOTS,)),
@@ -538,13 +560,12 @@
             dma((LAYERS,)),
             dma(()),
             dma(()),
-            dma(()),
         ],
         compiler_params=pltpu.CompilerParams(
-            collective_id=0, has_side_effects=True, vmem_limit_bytes=60 * 1024 * 1024
+            collective_id=0, has_side_effects=True, vmem_limit_bytes=40 * 1024 * 1024
         ),
         cost_estimate=pl.CostEstimate(flops=7 * 10**9, bytes_accessed=10**7, transcendentals=0),
-    )(stream, mix_weight, norm_gain, branch_scale)
+    )(*(pltpu.with_memory_space_constraint(v, pltpu.HBM) for v in (stream, mix_weight, norm_gain, branch_scale)))
 
 
 def solution(mesh):

time: 105 us -> 93.9 us (0.89)
  Pallas kernels: 101 us -> 92.2 us
  local copies, waits for them, and re-layouts: 3.91 us -> 1.67 us
    pallas_call x1, Pallas kernels: 101 us -> 92.2 us  [per_device(): pl.pallas_call(kernel, out_shape=jax.ShapeDtypeStruct((own_rows, width),...]
    unnamed x1, local copies, waits for them, and re-layouts: 3.91 us -> 1.67 us
where the time goes in v2:
time: 93.9 us
  Pallas kernels  92.2 us (98%)
  local copies, waits for them, and re-layouts  1.67 us (2%)
    pallas_call x1, Pallas kernels, per_device(): pl.pallas_call(kernel, out_shape=jax.ShapeDtypeStruct((own_rows, width),...  92.2 us

profile of v2, /device:TPU:33, one launch (start us, length us, event | category | flops | bytes accessed | tf_op | source)
XLA Modules:
  0.0 93.9 jit_solution(3520981820745018951)
XLA Ops:
  0.0 92.2 %shard_map.46 = bf16[384,4096]{1,0:T(8,128)(2,1)S(1)} custom-call(bf16[384,4096]{1,0:T(8,128)(2,1)} %stream.1, bf16[2,4,64,128]{3,2,1,0:T(8,128)(2,1)} %mixw.1, f32[2,4096]{1,0:T(2,128)} %gain_hbm.1, f32[2,4096]{1,0:T(2,128)} %bscale_hbm.1), custom_call_target="tpu_custom_call" | custom-call | flops 7000000000 | bytes 10000000 | tf_op jit(solution)/shard_map/pallas_call | solution.py:517
  92.2 1.7 %copy.6 = bf16[384,4096]{1,0:T(8,128)(2,1)} copy(bf16[384,4096]{1,0:T(8,128)(2,1)S(1)} %shard_map.46) | data formatting | bytes 6291456

commit v3 on v2

--- a/solution.py
+++ b/solution.py
@@ -20,7 +20,10 @@
 RING = 16
 SIDE = 4
 CW, CCW = 0, 1
-OFFSET = 4
+START_A = (0, 2)
+START_B = ((0, 1, 1, 2), (2, 5, 5, 6))
+FLIP = (0, 1, 3, 2)
+PIECES = ((0, 80),)
 SPLIT = 80
 BLOCK = 112
 BLOCK_SKIP = 16
@@ -145,9 +148,11 @@
     def part_b(l, xx, zz):
         return W.at[l, xx, zz, pl.ds(SPLIT, SLOTS * depth - SPLIT), :]
 
-    def pair_b(l, sub, zz):
-        half = x // 2 if sub == 0 else 1 - x // 2
-        return W.at[l, pl.ds(2 * half, 2), zz, pl.ds(SPLIT, SLOTS * depth - SPLIT), :]
+    def slab_b(l, k, zz):
+        return part_b(l, lax.bitwise_xor(x, FLIP[k]), zz)
+
+    def piece_a(l, p, zz):
+        return W.at[l, x, zz, pl.ds(*PIECES[p]), :]
 
     def x_sends(l, d, r, src):
         if d == CW:
@@ -167,14 +172,16 @@
 
         @pl.when((r >= 1) & (r <= end))
         def _():
-            src = part_a(l, x, source_z(d, r))
-            arrived(src, zA.at[l, d, r - 1])
-
-            @pl.when(r < end)
-            def _():
-                send(src, src, s_zA.at[l], zA.at[l, d, r], at_z(d))
-
-            x_sends(l, d, r, src)
+            zz = source_z(d, r)
+            for p in range(len(PIECES)):
+                src = piece_a(l, p, zz)
+                arrived(src, zA.at[l, p, d, r - 1])
+
+                @pl.when(r < end)
+                def _():
+                    send(src, src, s_zA.at[l], zA.at[l, p, d, r], at_z(d))
+
+            x_sends(l, d, r, part_a(l, x, zz))
 
     def on_xf(l, d, r):
         first = 1 if d == major(l) else 0
@@ -185,22 +192,24 @@
             arrived(src, xF.at[l, d, r])
             send(src, src, s_xA.at[l], xS.at[l], at_x(1 if d == CW else -1))
 
-    def on_b(l, sub, d, r):
-        end = last if d == sub else last - 1
+    def on_b(l, k, d, r):
+        end = last if d == k % 2 else last - 1
 
         @pl.when((r >= 1) & (r <= end))
         def _():
-            src = pair_b(l, sub, source_z(d, r))
-            arrived(src, zB.at[l, sub, d, r - 1])
+            src = slab_b(l, k, source_z(d, r))
+            arrived(src, zB.at[l, k, d, r - 1])
 
             @pl.when(r < end)
             def _():
-                send(src, src, s_zB.at[l], zB.at[l, sub, d, r], at_z(d))
+                send(src, src, s_zB.at[l], zB.at[l, k, d, r], at_z(d))
 
     def first_a(l):
         src = part_a(l, x, z)
-        for d in (CW, CCW):
-            send(src, src, s_zA.at[l], zA.at[l, d, 0], at_z(d))
+        for p in range(len(PIECES)):
+            for d in (CW, CCW):
+                piece = piece_a(l, p, z)
+                send(piece, piece, s_zA.at[l], zA.at[l, p, d, 0], at_z(d))
         x_sends(l, 1 - major(l), 0, src)
 
     def first_bx(l):
@@ -211,17 +220,17 @@
     def on_bx(l):
         from_left = part_b(l, ring_x(-1), z)
         from_right = part_b(l, ring_x(1), z)
+        arrived(from_right, bX.at[l, CCW])
+        if l == 0:
+            send(from_right, from_right, s_xB.at[l], bS.at[l], at_x(-1))
         arrived(from_left, bX.at[l, CW])
-        if l == 0:
+        if l == 1:
             send(from_left, from_left, s_xB.at[l], bS.at[l], at_x(1))
-        arrived(from_right, bX.at[l, CCW])
-        if l == 1:
-            send(from_right, from_right, s_xB.at[l], bS.at[l], at_x(-1))
-
-    def first_b(l, sub):
-        src = pair_b(l, sub, z)
+
+    def first_b(l, k):
+        src = slab_b(l, k, z)
         for d in (CW, CCW):
-            send(src, src, s_zB.at[l], zB.at[l, sub, d, 0], at_z(d))
+            send(src, src, s_zB.at[l], zB.at[l, k, d, 0], at_z(d))
 
     def on_bs(l):
         far = part_b(l, ring_x(2), z)
@@ -235,6 +244,7 @@
         first_bx(l)
         if l == 0:
             first_a(0)
+            first_b(0, 0)
 
     for s in range(SLOTS):
         peer_cols[s].wait()
@@ -386,7 +396,7 @@
 
         lax.fori_loop(start, stop, body, 0)
 
-    full = 2 + last
+    full, full1 = (max(START_A[l] + 2, *START_B[l]) + last for l in range(LAYERS))
 
     def filler(g, spot):
         if spot == 0:
@@ -412,76 +422,74 @@
         start = jnp.where(start < 0, rows // BLOCK, start)
         pool_many(start, jnp.minimum(start + 2, rows // BLOCK))
 
-        for l in range(LAYERS):
-            done = full + l * OFFSET
-            if spot == 2:
-                @pl.when(g == done - 1)
-                def _(l=l):
-                    mix_many(l, 0, SLOTS)
-
-                @pl.when(g == done)
-                def _(l=l):
-                    mix_many(l, 2 * SLOTS, 3 * SLOTS)
-                    finish_gather(l, 2)
-                    mix_many(l, 3 * SLOTS, 4 * SLOTS)
-                    if l == 0:
+        for l, at, where, k, slabs, hop in (
+            (0, full - 2, 2, 0, 1, 0), (0, full - 1, 2, 1, 1, 1), (0, full, 0, 2, 1, 0), (0, full, 2, 3, 1, 2),
+            (1, full1 - 1, 1, 0, 1, 0), (1, full1 - 1, 2, 1, 1, 1), (1, full1, 0, 2, 1, 0), (1, full1, 2, 3, 1, 2),
+        ):
+            if where == spot:
+                @pl.when(g == at)
+                def _(l=l, k=k, slabs=slabs, hop=hop):
+                    if hop:
+                        finish_gather(l, hop)
+                    mix_many(l, SLOTS * k, SLOTS * (k + slabs))
+                    if l == 0 and hop == 2:
                         send_ss(1)
-
-            if spot == 0:
-                @pl.when(g == done)
-                def _(l=l):
-                    finish_gather(l, 1)
-                    mix_many(l, SLOTS, 2 * SLOTS)
 
     def step(g, carry):
         for l in range(LAYERS):
             for d in (CW, CCW):
-                on_a(l, d, g - l * OFFSET)
-
-        @pl.when(g == OFFSET)
+                on_a(l, d, g - START_A[l])
+
+        @pl.when(g == START_A[1])
         def _():
             first_a(1)
 
-        @pl.when(g == 1)
+        def begin(l, *lanes):
+            for k in lanes:
+                @pl.when(g == START_B[l][k])
+                def _(k=k):
+                    first_b(l, k)
+
+        @pl.when(g == START_B[0][1])
         def _():
             on_bx(0)
-            first_b(0, 0)
-
+
+        begin(0, 1, 2)
+
+        @pl.when(g == START_B[0][3])
+        def _():
+            on_bs(0)
+
+        begin(1, 0)
         filler(g, 0)
+        for k in (0, 1):
+            for l in range(LAYERS):
+                for d in (CW, CCW):
+                    on_b(l, k, d, g - START_B[l][k])
         for l in range(LAYERS):
             for d in (CW, CCW):
-                on_b(l, 0, d, g - l * OFFSET - 1)
-        for l in range(LAYERS):
-            for d in (CW, CCW):
-                on_xf(l, d, g - l * OFFSET - 1)
-
-        @pl.when(g == 2)
-        def _():
-            on_bs(0)
-            first_b(0, 1)
+                on_xf(l, d, g - START_A[l] - 1)
+        begin(0, 3)
+        begin(1, 1, 2)
+        filler(g, 1)
+        for k in (2, 3):
+            for l in range(LAYERS):
+                for d in (CW, CCW):
+                    on_b(l, k, d, g - START_B[l][k])
 
         @pl.when(g == 3)
         def _():
             on_bx(1)
 
-        @pl.when(g == OFFSET + 1)
-        def _():
-            first_b(1, 0)
-
-        filler(g, 1)
-        for l in range(LAYERS):
-            for d in (CW, CCW):
-                on_b(l, 1, d, g - l * OFFSET - 2)
-
-        @pl.when(g == OFFSET + 2)
+        @pl.when(g == 5)
         def _():
             on_bs(1)
-            first_b(1, 1)
-
+
+        begin(1, 3)
         filler(g, 2)
         return carry
 
-    lax.fori_loop(1, OFFSET + full + 1, step, 0)
+    lax.fori_loop(1, full1 + 1, step, 0)
 
     for l in range(LAYERS):
         arrived(W.at[l, 0, pl.ds(0, RING - 1), pl.ds(0, SPLIT), :], s_zA.at[l])
@@ -543,8 +551,8 @@
             dma((SLOTS,)),
             dma((SLOTS,)),
             dma((LAYERS,)),
-            dma((LAYERS, 2, last)),
-            dma((LAYERS, 2, 2, last)),
+            dma((LAYERS, len(PIECES), 2, last)),
+            dma((LAYERS, SIDE, 2, last)),
             dma((LAYERS, 2, last + 1)),
             dma((LAYERS, 2)),
             dma((LAYERS,)),

time: 93.9 us -> 92.7 us (0.987)
  Pallas kernels: 92.2 us -> 90.9 us
    pallas_call x1, Pallas kernels: 92.2 us -> 90.9 us  [per_device(): pl.pallas_call(kernel, out_shape=jax.ShapeDtypeStruct((own_rows, width),...]
where the time goes in v3:
time: 92.7 us; the launch traced here: 92.6 us
  Pallas kernels  90.9 us (98%)
  local copies, waits for them, and re-layouts  1.67 us (2%)
    pallas_call x1, Pallas kernels, per_device(): pl.pallas_call(kernel, out_shape=jax.ShapeDtypeStruct((own_rows, width),...  90.9 us

profile of v3, /device:TPU:33, one launch (start us, length us, event | category | flops | bytes accessed | tf_op | source)
XLA Modules:
  0.0 92.6 jit_solution(2277467109759697720)
XLA Ops:
  0.0 90.9 %shard_map.46 = bf16[384,4096]{1,0:T(8,128)(2,1)S(1)} custom-call(bf16[384,4096]{1,0:T(8,128)(2,1)} %stream.1, bf16[2,4,64,128]{3,2,1,0:T(8,128)(2,1)} %mixw.1, f32[2,4096]{1,0:T(2,128)} %gain_hbm.1, f32[2,4096]{1,0:T(2,128)} %bscale_hbm.1), custom_call_target="tpu_custom_call" | custom-call | flops 7000000000 | bytes 10000000 | tf_op jit(solution)/shard_map/pallas_call | solution.py:525
  90.9 1.7 %copy.6 = bf16[384,4096]{1,0:T(8,128)(2,1)} copy(bf16[384,4096]{1,0:T(8,128)(2,1)S(1)} %shard_map.46) | data formatting | bytes 6291456

commit v4 on v3

--- a/solution.py
+++ b/solution.py
@@ -462,8 +462,8 @@
 
         begin(1, 0)
         filler(g, 0)
-        for k in (0, 1):
-            for l in range(LAYERS):
+        for l in range(LAYERS):
+            for k in (0, 1):
                 for d in (CW, CCW):
                     on_b(l, k, d, g - START_B[l][k])
         for l in range(LAYERS):
@@ -472,8 +472,8 @@
         begin(0, 3)
         begin(1, 1, 2)
         filler(g, 1)
-        for k in (2, 3):
-            for l in range(LAYERS):
+        for l in range(LAYERS):
+            for k in (2, 3):
                 for d in (CW, CCW):
                     on_b(l, k, d, g - START_B[l][k])
 

time: 92.7 us -> 92.7 us (level)
  no operation moved by 1% of the time
where the time goes in v4:
time: 92.7 us; the launch traced here: 92.6 us
  Pallas kernels  90.9 us (98%)
  local copies, waits for them, and re-layouts  1.67 us (2%)
    pallas_call x1, Pallas kernels, per_device(): pl.pallas_call(kernel, out_shape=jax.ShapeDtypeStruct((own_rows, width),...  90.9 us

profile of v4, /device:TPU:33, one launch (start us, length us, event | category | flops | bytes accessed | tf_op | source)
XLA Modules:
  0.0 92.6 jit_solution(16390497393703140929)
XLA Ops:
  0.0 90.9 %shard_map.46 = bf16[384,4096]{1,0:T(8,128)(2,1)S(1)} custom-call(bf16[384,4096]{1,0:T(8,128)(2,1)} %stream.1, bf16[2,4,64,128]{3,2,1,0:T(8,128)(2,1)} %mixw.1, f32[2,4096]{1,0:T(2,128)} %gain_hbm.1, f32[2,4096]{1,0:T(2,128)} %bscale_hbm.1), custom_call_target="tpu_custom_call" | custom-call | flops 7000000000 | bytes 10000000 | tf_op jit(solution)/shard_map/pallas_call | solution.py:525
  90.9 1.7 %copy.6 = bf16[384,4096]{1,0:T(8,128)(2,1)} copy(bf16[384,4096]{1,0:T(8,128)(2,1)S(1)} %shard_map.46) | data formatting | bytes 6291456
